TPU v7x, 256 devices: a 2x2x32 block of a 4x8x32 slice. The times are simulated.
256 devices in a mesh: grp: 4 (over y, x), ep: 64 (over z, core).
Axes of the slice: x: 2, y: 2, z: 32, core: 2. Of those that a mesh axis runs over, the one named last changes fastest.
The devices are a block of a 4x8x32 slice.
Arguments:
- tokens: bfloat16 [256, 2048], P(('grp', 'ep')), parts along dimension 0, may hold values from -6 to 6
- cache_latent: bfloat16 [256, 3072, 512], P(('grp', 'ep')), parts along dimension 0, may hold values from -6 to 6
- cache_rope: bfloat16 [256, 32, 3072], P(('grp', 'ep')), parts along dimension 0, may hold values from -1000 to 1000
- lengths: int32 [256], P(('grp', 'ep')), parts along dimension 0, may hold values from 384 to 3072, as said below
- w_query: bfloat16 [2048, 1536], P('ep'), may hold values from -0.125 to 0.125
- w_latent: bfloat16 [2048, 512], P('ep'), may hold values from -0.125 to 0.125
- w_rope: bfloat16 [2048, 32], P('ep'), may hold values from -0.125 to 0.125
- w_absorb: bfloat16 [512, 1024], replicated, may hold values from -0.25 to 0.25
- w_value: bfloat16 [512, 1024], replicated, may hold values from -0.25 to 0.25
- w_output: bfloat16 [1024, 2048], P('ep'), may hold values from -0.1875 to 0.1875
- gain_attn: float32 [2048], replicated, may hold values from 0.1 to 1.9
- gain_latent: float32 [512], replicated, may hold values from 0.1 to 1.9
- gain_moe: float32 [2048], replicated, may hold values from 0.1 to 1.9
- routes: int32 [256, 2], P(('grp', 'ep')), parts along dimension 0, may hold values from 0 to 63, all different within a row; in each aligned block of 64 rows (0 to 63, 64 to 127, ...) at most 4 rows name the same one
- route_scores: float32 [256, 2], P(('grp', 'ep')), parts along dimension 0, may hold values from 0.2 to 1
- w_gate: bfloat16 [64, 2048, 512], P('ep'), may hold values from -0.125 to 0.125
- w_up: bfloat16 [64, 2048, 512], P('ep'), may hold values from -0.125 to 0.125
- w_down: bfloat16 [64, 512, 2048], P('ep'), may hold values from -0.25 to 0.25
Outputs:
- mixed: bfloat16 [256, 2048], P(('grp', 'ep')), parts along dimension 0
- new_latent: bfloat16 [256, 512], P(('grp', 'ep')), parts along dimension 0
- new_rope: bfloat16 [256, 32], P(('grp', 'ep')), parts along dimension 0
There are 4 independent parts, one for each index of `grp`. A program takes and returns all parts, laid end to end along the dimension named above; an argument that names none is the same for every part. Nothing has to cross between parts.
Inputs may be any that keep to these rules, and one draw needn't show every extreme that they name: `routes`: each row names 2 different experts; over one part's 64 tokens no expert is named by more than 4 rows, a bound that some block reaches. `lengths`: some sequence has all 3072 positions filled.
All inputs are finite; a program needn't handle non-finite values.
Results may differ from a plain program's by a relative error of at most 0.013.
Values may be sent and summed in bfloat16 or wider, within the bound.
A program may use at most 64 MiB of HBM per device.

v0:
```python
import jax
import jax.numpy as jnp
from jax import lax
from jax.sharding import PartitionSpec as P

D = 2048
HEADS = 16
NOPE = 64
ROPE = 32
VDIM = 64
LATENT = 512
CAP = 4


EPS = 1e-06
THETA = 10000.0


def in_blocks(shard, dim, devices):
    before, after = (shard.shape[:dim], shard.shape[dim + 1 :])
    return jnp.moveaxis(shard.reshape(*before, devices, -1, *after), dim, 0)


def summed_on_arrival(shard, axis, dim):
    tiles = in_blocks(shard, dim, lax.axis_size(axis))
    arrived = lax.all_to_all(tiles, axis, split_axis=0, concat_axis=0, tiled=True)
    return arrived.sum(axis=0)


def sent_and_summed(shard, axis, dim):
    tiles = in_blocks(shard, dim, lax.axis_size(axis))
    arrived = lax.all_to_all(tiles, axis, split_axis=0, concat_axis=0, tiled=True)
    return arrived.astype(jnp.float32).sum(axis=0)


def rms_scale(values, gain):
    return values * lax.rsqrt(jnp.mean(values * values, axis=-1, keepdims=True) + EPS) * gain


def rope_tables(positions, width):
    inverse = THETA ** (-jnp.arange(0, width, 2).astype(jnp.float32) / width)
    angle = positions.astype(jnp.float32)[:, None] * inverse[None, :]
    return (jnp.cos(angle), jnp.sin(angle))


def apply_rope(values, cosine, sine):
    half = values.shape[-1] // 2
    first, second = (values[..., :half], values[..., half:])
    return jnp.concatenate(
        [first * cosine - second * sine, second * cosine + first * sine], axis=-1
    )


def body(
    tokens,
    cache_latent,
    cache_rope,
    lengths,
    w_query,
    w_latent,
    w_rope,
    w_absorb,
    w_value,
    w_output,
    gain_attn,
    gain_latent,
    gain_moe,
    routes,
    route_scores,
    w_gate,
    w_up,
    w_down,
):
    local_seqs = tokens.shape[0]
    devices = lax.axis_size("ep")
    q_width = w_query.shape[1]
    lat_width = w_latent.shape[1]
    normed = rms_scale(tokens.astype(jnp.float32), gain_attn).astype(jnp.bfloat16)
    feature_rows = lax.all_to_all(normed, "ep", split_axis=1, concat_axis=0, tiled=True)
    stacked = jnp.concatenate([w_query, w_latent, w_rope], axis=1)
    rows = feature_rows
    summed = summed_on_arrival(jnp.dot(rows, stacked, preferred_element_type=jnp.float32), "ep", 0)
    query = summed[:, :q_width].astype(jnp.bfloat16)
    latent_raw = summed[:, q_width : q_width + lat_width].astype(jnp.bfloat16)
    rope_raw = summed[:, q_width + lat_width :].astype(jnp.bfloat16)
    new_latent = rms_scale(latent_raw.astype(jnp.float32), gain_latent).astype(jnp.bfloat16)
    cosine, sine = rope_tables(lengths, ROPE)
    new_rope = apply_rope(rope_raw.astype(jnp.float32), cosine, sine).astype(jnp.bfloat16)
    heads_view = query.reshape(local_seqs, HEADS, NOPE + ROPE)
    q_nope = heads_view[:, :, :NOPE]
    q_pe = apply_rope(
        heads_view[:, :, NOPE:].astype(jnp.float32), cosine[:, None, :], sine[:, None, :]
    ).astype(jnp.bfloat16)
    q_abs = jnp.einsum(
        "shn,chn->shc",
        q_nope,
        w_absorb.reshape(LATENT, HEADS, NOPE),
        preferred_element_type=jnp.float32,
    ).astype(jnp.bfloat16)
    scale = (NOPE + ROPE) ** (-0.5)
    past = (
        jnp.einsum("shc,skc->shk", q_abs, cache_latent, preferred_element_type=jnp.float32)
        + jnp.einsum("shr,srk->shk", q_pe, cache_rope, preferred_element_type=jnp.float32)
    ) * scale
    fresh = (
        jnp.einsum("shc,sc->sh", q_abs, new_latent, preferred_element_type=jnp.float32)
        + jnp.einsum("shr,sr->sh", q_pe, new_rope, preferred_element_type=jnp.float32)
    ) * scale
    valid = jnp.arange(cache_latent.shape[1])[None, None, :] < lengths[:, None, None]
    top = jnp.maximum(jnp.max(jnp.where(valid, past, -jnp.inf), axis=-1), fresh)
    e_past = jnp.where(valid, jnp.exp(past - top[:, :, None]), 0.0)
    e_new = jnp.exp(fresh - top)
    total = jnp.sum(e_past, axis=-1) + e_new
    p_past = (e_past / total[:, :, None]).astype(jnp.bfloat16)
    p_new = (e_new / total).astype(jnp.bfloat16)
    attended = (
        jnp.einsum("shk,skc->shc", p_past, cache_latent, preferred_element_type=jnp.float32)
        + p_new.astype(jnp.float32)[:, :, None] * new_latent.astype(jnp.float32)[:, None, :]
    ).astype(jnp.bfloat16)
    values = jnp.einsum(
        "shc,chv->shv",
        attended,
        w_value.reshape(LATENT, HEADS, VDIM),
        preferred_element_type=jnp.float32,
    ).astype(jnp.bfloat16)
    values = values.reshape(local_seqs, HEADS * VDIM)
    head_rows = lax.all_to_all(values, "ep", split_axis=1, concat_axis=0, tiled=True)
    rows = head_rows
    attn_out = sent_and_summed(
        jnp.dot(rows, w_output, preferred_element_type=jnp.float32).astype(jnp.bfloat16), "ep", 0
    )
    resid = (tokens.astype(jnp.float32) + attn_out).astype(jnp.bfloat16)
    moe_in = rms_scale(resid.astype(jnp.float32), gain_moe).astype(jnp.bfloat16)
    route_weight = route_scores / jnp.sum(route_scores, axis=-1, keepdims=True)
    slots = jnp.arange(CAP).astype(jnp.float32)
    expert_ids = jnp.arange(devices)
    hits = routes[:, :, None] == expert_ids[None, None, :]
    chosen = jnp.any(hits, axis=1)
    outgoing = jnp.where(chosen.T[:, :, None], moe_in[None, :, :], jnp.zeros((), jnp.bfloat16))
    flags_out = chosen.T.astype(jnp.bfloat16)
    arrived, arrived_flags = (
        lax.all_to_all(outgoing, "ep", split_axis=0, concat_axis=0, tiled=True),
        lax.all_to_all(flags_out, "ep", split_axis=0, concat_axis=0, tiled=True),
    )
    flat_rows = arrived.reshape(devices * local_seqs, D)
    flag = arrived_flags.reshape(-1).astype(jnp.float32)
    rank = jnp.cumsum(flag) - 1.0
    picker = ((rank[None, :] == slots[:, None]) & (flag[None, :] > 0.5)).astype(jnp.bfloat16)
    packed = jnp.dot(picker, flat_rows, preferred_element_type=jnp.float32).astype(jnp.bfloat16)
    gate = jnp.dot(packed, w_gate[0], preferred_element_type=jnp.float32)
    upper = jnp.dot(packed, w_up[0], preferred_element_type=jnp.float32)
    hidden = (jax.nn.silu(gate) * upper).astype(jnp.bfloat16)
    result = jnp.dot(hidden, w_down[0], preferred_element_type=jnp.float32).astype(jnp.bfloat16)
    spread = (
        jnp.dot(picker.T, result, preferred_element_type=jnp.float32)
        .astype(jnp.bfloat16)
        .reshape(devices, local_seqs, D)
    )
    answers = lax.all_to_all(spread, "ep", split_axis=0, concat_axis=0, tiled=True)
    weight_table = jnp.sum(hits.astype(jnp.float32) * route_weight[:, :, None], axis=1)
    moe_sum = jnp.einsum("sn,nsd->sd", weight_table, answers.astype(jnp.float32))
    mixed = (resid.astype(jnp.float32) + moe_sum).astype(jnp.bfloat16)
    return (mixed, new_latent, new_rope)


def solution(mesh):
    placed = (
        P(("grp", "ep"), None),
        P(("grp", "ep"), None, None),
        P(("grp", "ep"), None, None),
        P(("grp", "ep")),
        P("ep", None),
        P("ep", None),
        P("ep", None),
        P(),
        P(),
        P("ep", None),
        P(),
        P(),
        P(),
        P(("grp", "ep"), None),
        P(("grp", "ep"), None),
        P("ep", None, None),
        P("ep", None, None),
        P("ep", None, None),
    )
    return jax.shard_map(
        body,
        mesh=mesh,
        in_specs=placed,
        out_specs=(P(("grp", "ep"), None), P(("grp", "ep"), None), P(("grp", "ep"), None)),
        check_vma=False,
    )
```

profile of v0, /device:TPU:46, one launch (start us, length us, event | category | flops | bytes accessed | tf_op | source)
XLA Modules:
  0.0 366.9 jit_solution(1477472683114162696)
XLA Ops:
  0.6 1.5 multiply_reduce_fusion.1
  3.6 56.0 %all_to_all.60 = bf16[1,64,32]{2,0,1:T(2,128)(2,1)S(1)} all-to-all(bf16[1,64,32]{2,0,1:T(2,128)(2,1)S(1)} %all_to_all.51), channel_id=1, replica_groups=mesh['grp'=4,'ep'=64] {'ep'}, dimensions={1} | all-to-all | bytes 8192 | tf_op jit(solution)/shard_map/all_to_all | solution.py:79
  59.8 1.2 convolution_bitcast_fusion
  61.0 1.4 copy.47
  62.4 7.1 %all-to-all-start.1 = ((f32[64,1,2080]{2,1,0:T(1,128)}), f32[64,1,2080]{2,1,0:T(1,128)}, u32[]{:S(2)}, u32[]{:S(2)}) async-start(f32[64,1,2080]{2,1,0:T(1,128)} %copy.47), calls=%async_computation.1 | async-start | bytes 1114112 | tf_op jit(solution)/shard_map/all_to_all | solution.py:26
  70.2 2.3 copy.48
  72.5 2.3 copy.49
  74.9 61.8 %all-to-all-done.1 = f32[64,1,2080]{2,1,0:T(1,128)} async-done(((f32[64,1,2080]{2,1,0:T(1,128)}), f32[64,1,2080]{2,1,0:T(1,128)}, u32[]{:S(2)}, u32[]{:S(2)}) %all-to-all-start.1) | async-done | bytes 532512 | tf_op jit(solution)/shard_map/all_to_all | solution.py:26
  136.6 1.4 reduce_sum.77
  139.7 1.5 fusion.50
  141.6 1.0 select_reduce_fusion
  144.3 27.7 %all_to_all.61 = bf16[1,64,16]{2,0,1:T(2,128)(2,1)S(1)} all-to-all(bf16[1,64,16]{2,0,1:T(2,128)(2,1)S(1)} %all_to_all.52), channel_id=1, replica_groups=mesh['grp'=4,'ep'=64] {'ep'}, dimensions={1} | all-to-all | bytes 4096 | tf_op jit(solution)/shard_map/all_to_all | solution.py:127
  172.9 1.4 reduce.24
  174.3 1.8 reshape.522
  176.1 6.5 %all-to-all-start.3 = ((bf16[64,2,1024]{2,1,0:T(2,128)(2,1)}), bf16[64,2,1024]{2,1,0:T(2,128)(2,1)S(1)}, u32[]{:S(2)}, u32[]{:S(2)}) async-start(bf16[64,2,1024]{2,1,0:T(2,128)(2,1)} %reshape.522), calls=%async_computation.3 | async-start | bytes 524288 | tf_op jit(solution)/shard_map/all_to_all | solution.py:32
  183.4 40.9 %all-to-all-done.3 = bf16[64,2,1024]{2,1,0:T(2,128)(2,1)S(1)} async-done(((bf16[64,2,1024]{2,1,0:T(2,128)(2,1)}), bf16[64,2,1024]{2,1,0:T(2,128)(2,1)S(1)}, u32[]{:S(2)}, u32[]{:S(2)}) %all-to-all-start.3) | async-done | bytes 262176 | tf_op jit(solution)/shard_map/all_to_all | solution.py:32
  224.4 6.7 %all-to-all-start.4 = ((bf16[64,1,1]{2,1,0:T(2,128)(2,1)}), bf16[64,1,1]{2,1,0:T(2,128)(2,1)S(1)}, u32[]{:S(2)}, u32[]{:S(2)}) async-start(bf16[64,1,1]{2,1,0:T(2,128)(2,1)} %copy.53), calls=%async_computation.4 | async-start | bytes 65536 | tf_op jit(solution)/shard_map/all_to_all | solution.py:143
  231.9 1.5 convert_reduce_fusion
  234.9 1.2 broadcast_select_fusion
  236.1 3.1 reduce.25
  240.1 12.9 %all-to-all-done.4 = bf16[64,1,1]{2,1,0:T(2,128)(2,1)S(1)} async-done(((bf16[64,1,1]{2,1,0:T(2,128)(2,1)}), bf16[64,1,1]{2,1,0:T(2,128)(2,1)S(1)}, u32[]{:S(2)}, u32[]{:S(2)}) %all-to-all-start.4) | async-done | bytes 160 | tf_op jit(solution)/shard_map/all_to_all | solution.py:143
  253.0 10.3 %all-to-all-start.5 = ((bf16[64,2,1024]{2,1,0:T(2,128)(2,1)}), bf16[64,2,1024]{2,1,0:T(2,128)(2,1)S(1)}, u32[]{:S(2)}, u32[]{:S(2)}) async-start(bf16[64,2,1024]{2,1,0:T(2,128)(2,1)} %reshape.524), calls=%async_computation.5 | async-start | bytes 524288 | tf_op jit(solution)/shard_map/all_to_all | solution.py:142
  263.6 1.2 compare_reduce_fusion
  264.8 40.3 %all-to-all-done.5 = bf16[64,2,1024]{2,1,0:T(2,128)(2,1)S(1)} async-done(((bf16[64,2,1024]{2,1,0:T(2,128)(2,1)}), bf16[64,2,1024]{2,1,0:T(2,128)(2,1)S(1)}, u32[]{:S(2)}, u32[]{:S(2)}) %all-to-all-start.5) | async-done | bytes 262176 | tf_op jit(solution)/shard_map/all_to_all | solution.py:142
  306.0 1.3 convolution_convert_fusion.3
  307.3 2.0 fusion.10
  309.3 3.0 convolution_convert_fusion.2
  312.6 1.4 reduce.26
  314.0 1.8 reshape.526
  315.9 6.5 %all-to-all-start.6 = ((bf16[64,2,1024]{2,1,0:T(2,128)(2,1)}), bf16[64,2,1024]{2,1,0:T(2,128)(2,1)S(1)}, u32[]{:S(2)}, u32[]{:S(2)}) async-start(bf16[64,2,1024]{2,1,0:T(2,128)(2,1)} %reshape.526), calls=%async_computation.6 | async-start | bytes 524288 | tf_op jit(solution)/shard_map/all_to_all | solution.py:159
  324.3 39.8 %all-to-all-done.6 = bf16[64,2,1024]{2,1,0:T(2,128)(2,1)S(1)} async-done(((bf16[64,2,1024]{2,1,0:T(2,128)(2,1)}), bf16[64,2,1024]{2,1,0:T(2,128)(2,1)S(1)}, u32[]{:S(2)}, u32[]{:S(2)}) %all-to-all-start.6) | async-done | bytes 262176 | tf_op jit(solution)/shard_map/all_to_all | solution.py:159
  365.0 1.9 fusion.6
  (66 shorter events, 12.5 us)
Async XLA Ops:
  0.6 140.9 %copy-start = (bf16[1,3072,512]{2,1,0:T(8,128)(2,1)S(1)}, bf16[1,3072,512]{2,1,0:T(8,128)(2,1)}, u32[]{:S(2)}) copy-start(bf16[1,3072,512]{2,1,0:T(8,128)(2,1)} %param.19) | copy-start | bytes 9437188
  62.4 74.3 %all-to-all-start.1 = ((f32[64,1,2080]{2,1,0:T(1,128)}), f32[64,1,2080]{2,1,0:T(1,128)}, u32[]{:S(2)}, u32[]{:S(2)}) async-start(f32[64,1,2080]{2,1,0:T(1,128)} %copy.47), calls=%async_computation.1 | async-start | bytes 1114112 | tf_op jit(solution)/shard_map/all_to_all | solution.py:26
  70.1 69.5 %copy-start.6 = (f32[512]{0:T(512)S(1)}, f32[512]{0:T(512)}, u32[]{:S(2)}) copy-start(f32[512]{0:T(512)} %param.29) | copy-start | bytes 6148
  72.5 68.9 %copy-start.2 = (bf16[1,32,3072]{2,1,0:T(8,128)(2,1)S(1)}, bf16[1,32,3072]{2,1,0:T(8,128)(2,1)}, u32[]{:S(2)}) copy-start(bf16[1,32,3072]{2,1,0:T(8,128)(2,1)} %param.20) | copy-start | bytes 589828
  139.6 3.0 copy-start.7
  142.6 1.2 copy-start.1
  143.1 29.0 %copy-start.4 = (bf16[16,2048]{1,0:T(8,128)(2,1)S(1)}, bf16[16,2048]{1,0:T(8,128)(2,1)}, u32[]{:S(2)}) copy-start(bf16[16,2048]{1,0:T(8,128)(2,1)} %param.27) | copy-start | bytes 196612
  143.7 39.0 %copy-start.9 = (s32[1,2]{1,0:T(1,128)S(1)}, s32[1,2]{1,0:T(1,128)}, u32[]{:S(2)}) copy-start(s32[1,2]{1,0:T(1,128)} %param.31) | copy-start | bytes 28
  143.9 89.6 %copy-start.3 = (bf16[1,2048]{1,0:T(2,128)(2,1)S(1)}, bf16[1,2048]{1,0:T(2,128)(2,1)}, u32[]{:S(2)}) copy-start(bf16[1,2048]{1,0:T(2,128)(2,1)} %param.18) | copy-start | bytes 12292
  143.9 91.0 %copy-start.5 = (f32[2048]{0:T(1024)S(1)}, f32[2048]{0:T(1024)}, u32[]{:S(2)}) copy-start(f32[2048]{0:T(1024)} %param.30) | copy-start | bytes 24580
  176.1 48.2 %all-to-all-start.3 = ((bf16[64,2,1024]{2,1,0:T(2,128)(2,1)}), bf16[64,2,1024]{2,1,0:T(2,128)(2,1)S(1)}, u32[]{:S(2)}, u32[]{:S(2)}) async-start(bf16[64,2,1024]{2,1,0:T(2,128)(2,1)} %reshape.522), calls=%async_computation.3 | async-start | bytes 524288 | tf_op jit(solution)/shard_map/all_to_all | solution.py:32
  224.4 28.6 %all-to-all-start.4 = ((bf16[64,1,1]{2,1,0:T(2,128)(2,1)}), bf16[64,1,1]{2,1,0:T(2,128)(2,1)S(1)}, u32[]{:S(2)}, u32[]{:S(2)}) async-start(bf16[64,1,1]{2,1,0:T(2,128)(2,1)} %copy.53), calls=%async_computation.4 | async-start | bytes 65536 | tf_op jit(solution)/shard_map/all_to_all | solution.py:143
  253.0 52.1 %all-to-all-start.5 = ((bf16[64,2,1024]{2,1,0:T(2,128)(2,1)}), bf16[64,2,1024]{2,1,0:T(2,128)(2,1)S(1)}, u32[]{:S(2)}, u32[]{:S(2)}) async-start(bf16[64,2,1024]{2,1,0:T(2,128)(2,1)} %reshape.524), calls=%async_computation.5 | async-start | bytes 524288 | tf_op jit(solution)/shard_map/all_to_all | solution.py:142
  309.3 13.1 %copy-start.8 = (f32[1,2]{1,0:T(1,128)S(1)}, f32[1,2]{1,0:T(1,128)}, u32[]{:S(2)}) copy-start(f32[1,2]{1,0:T(1,128)} %param.32) | copy-start | bytes 28
  315.9 48.2 %all-to-all-start.6 = ((bf16[64,2,1024]{2,1,0:T(2,128)(2,1)}), bf16[64,2,1024]{2,1,0:T(2,128)(2,1)S(1)}, u32[]{:S(2)}, u32[]{:S(2)}) async-start(bf16[64,2,1024]{2,1,0:T(2,128)(2,1)} %reshape.526), calls=%async_computation.6 | async-start | bytes 524288 | tf_op jit(solution)/shard_map/all_to_all | solution.py:159
where the time goes:
time: 369 us; the launch traced here: 367 us
  waiting for transfers between devices  196 us (53%)
  blocking collectives  83.7 us (23%)
  starting transfers between devices  37.1 us (10%)
  other arithmetic  17.7 us (5%)
  local copies, waits for them, and re-layouts  15.3 us (4%)
  matrix products  13.9 us (4%)
    all_to_all x1, waiting for transfers between devices, summed_on_arrival(): lax.all_to_all(tiles, axis, split_axis=0, concat_axis=0, tiled=True)  61.8 us
    all_to_all x1, blocking collectives, body(): lax.all_to_all(normed, 'ep', split_axis=1, concat_axis=0, tiled=True)  56 us
    all_to_all x1, waiting for transfers between devices, sent_and_summed(): lax.all_to_all(tiles, axis, split_axis=0, concat_axis=0, tiled=True)  40.9 us
    all_to_all x1, waiting for transfers between devices, body(): lax.all_to_all(outgoing, 'ep', split_axis=0, concat_axis=0, tiled=True)  40.3 us
    all_to_all x1, waiting for transfers between devices, body(): lax.all_to_all(spread, 'ep', split_axis=0, concat_axis=0, tiled=True)  39.8 us
    all_to_all x1, blocking collectives, body(): lax.all_to_all(values, 'ep', split_axis=1, concat_axis=0, tiled=True)  27.7 us
    all_to_all x1, waiting for transfers between devices, body(): lax.all_to_all(flags_out, 'ep', split_axis=0, concat_axis=0, tiled=True)  12.9 us
    unnamed x28, local copies, waits for them, and re-layouts  12.2 us
  transfers between devices with their start and end apart: 5, of which 5 were waited for; matrix products, arithmetic and copies ran while one was open for 5% of the time, Pallas kernels for 0%

commit v1 on v0

v1 whole, which is shorter than its diff:
```python
import functools

import jax
import jax.numpy as jnp
from jax import lax
from jax.experimental import pallas as pl
from jax.experimental.pallas import tpu as pltpu
from jax.sharding import PartitionSpec as P

HEADS = 16
NOPE = 64
ROPE = 32
VDIM = 64
LATENT = 512
EPS = 1e-06
THETA = 10000.0
MESH = pl.DeviceIdType.MESH
F32 = jnp.float32
BF16 = jnp.bfloat16


def rope_tables(positions, width):
    inverse = THETA ** (-jnp.arange(0, width, 2).astype(F32) / width)
    angle = positions.astype(F32)[:, None] * inverse[None, :]
    return (jnp.cos(angle), jnp.sin(angle))


def farthest_first(i, n):
    half = (i + 1) // 2
    return n // 2 + half * (1 - 2 * lax.rem(i, 2))


def rotate(x, cosine, sine):
    lanes = x.shape[-1]
    place = lax.rem(lax.broadcasted_iota(jnp.int32, x.shape, 1), ROPE)
    ahead = pltpu.roll(x, lanes - ROPE // 2, 1)
    behind = pltpu.roll(x, ROPE // 2, 1)
    return jnp.where(place < ROPE // 2, x * cosine - ahead * sine, x * cosine + behind * sine)


def dot(a, b):
    return jnp.dot(a, b, preferred_element_type=F32)


def dot_nt(a, b):
    return lax.dot_general(a, b, (((1,), (1,)), ((), ())), preferred_element_type=F32)


def kernel(
    nz,
    length_ref,
    tokens_hbm,
    cache_hbm,
    rope_hbm,
    wq_hbm,
    wl_hbm,
    wr_hbm,
    wa_hbm,
    wv_hbm,
    wo_hbm,
    gain_attn_hbm,
    gain_latent_hbm,
    gain_moe_hbm,
    cos_hbm,
    sin_hbm,
    wt_hbm,
    wg_hbm,
    wu_hbm,
    wd_hbm,
    mixed_ref,
    new_latent_ref,
    new_rope_ref,
    tokens_v,
    gain_attn_v,
    gain_latent_v,
    gain_moe_v,
    cos_v,
    sin_v,
    wt_v,
    cache_v,
    rope_v,
    wa_v,
    wv_v,
    wq_v,
    wl_v,
    wr_v,
    wo_v,
    wg_v,
    wu_v,
    wd_v,
    p1_send,
    p1_recv,
    wt_recv,
    p2_send,
    p2_recv,
    p3_send,
    p3_recv,
    x3,
    c4,
    p4_send,
    p4_recv,
    local_sem,
    send16,
    send32,
    sendw,
    p1_sem,
    wt_sem,
    p2_sem,
    p3_sem,
    p4_sem,
    w_send,
    w_recv,
    e_send,
    e_recv,
    right_send,
    right_recv,
    left_send,
    left_recv,
    part_send,
    part_recv,
):
    g = lax.axis_index("grp")
    e = lax.axis_index("ep")
    z = e // 2
    c = lax.rem(e, 2)
    m = z // 2
    p = lax.rem(z, 2)
    nm = nz // 2
    q_width = wq_hbm.shape[1]
    lat = wl_hbm.shape[1]
    ropes = wr_hbm.shape[1]
    fper = wq_hbm.shape[0]
    feats = 4 * fper
    d_model = tokens_hbm.shape[1]
    half = d_model // 2
    cache = cache_v.shape[0]

    def dev(zz, cc):
        return (g, zz * 2 + cc)

    beside = z + 1 - 2 * p
    right = lax.rem(z + 1, nz)
    left = lax.rem(z + nz - 1, nz)

    def remote(src, dst, send, recv, to):
        return pltpu.make_async_remote_copy(
            src_ref=src, dst_ref=dst, send_sem=send, recv_sem=recv, device_id=to, device_id_type=MESH
        )

    barrier = pltpu.get_barrier_semaphore()

    def greet(i, _):
        pl.semaphore_signal(barrier, inc=1, device_id=dev(lax.rem(z + i, nz), c), device_id_type=MESH)
        return 0

    lax.fori_loop(1, nz, greet, 0)
    pl.semaphore_signal(barrier, inc=1, device_id=dev(z, 1 - c), device_id_type=MESH)
    pl.semaphore_signal(barrier, inc=1, device_id=dev(beside, 1 - c), device_id_type=MESH)

    block = 2 * p + c
    rows = pl.ds(pl.multiple_of(block * fper, fper), fper)
    loads = [
        (tokens_hbm, tokens_v),
        (gain_attn_hbm, gain_attn_v),
        (wt_hbm, wt_v),
        (wq_hbm, wq_v.at[rows]),
        (wl_hbm, wl_v.at[rows]),
        (wr_hbm, wr_v.at[rows]),
        (gain_latent_hbm, gain_latent_v),
        (gain_moe_hbm, gain_moe_v),
        (cos_hbm, cos_v),
        (sin_hbm, sin_v),
        (wo_hbm, wo_v.at[e]),
        (wa_hbm, wa_v),
        (cache_hbm.at[0], cache_v),
        (rope_hbm.at[0], rope_v),
        (wv_hbm, wv_v),
        (wg_hbm.at[0], wg_v.at[c]),
        (wu_hbm.at[0], wu_v.at[c]),
        (wd_hbm.at[0], wd_v.at[c]),
    ]
    local = [pltpu.make_async_copy(a, b, local_sem.at[i]) for i, (a, b) in enumerate(loads)]
    for copy in local:
        copy.start()

    local[0].wait()
    local[1].wait()
    local[2].wait()
    tokens = tokens_v[...].astype(F32)
    normed = tokens * lax.rsqrt(jnp.mean(tokens * tokens, axis=-1, keepdims=True) + EPS) * gain_attn_v[...]
    normed = normed.astype(BF16).astype(F32)
    for i in range(nm):
        p1_send[i] = normed[:, i * feats : (i + 1) * feats]
    p1_recv[m] = p1_send[m]
    wt_recv[z] = wt_v[...]
    p2_send[...] = jnp.zeros_like(p2_send)

    pl.semaphore_wait(barrier, nz + 1)

    def p1_copy(to, slot, d):
        return remote(p1_send.at[to], p1_recv.at[slot], send16.at[d], p1_sem.at[slot], dev(2 * to + p, c))

    def p1_start(i, _):
        d = farthest_first(i, nm)
        p1_copy(lax.rem(m + d, nm), m, d).start()
        return 0

    lax.fori_loop(0, nm - 1, p1_start, 0)

    w_pairs = ((wq_hbm, wq_v), (wl_hbm, wl_v), (wr_hbm, wr_v))
    w_targets = (dev(beside, c), dev(beside, 1 - c), dev(z, 1 - c))

    def w_copies(slot, k):
        at = pl.ds(pl.multiple_of(slot * fper, fper), fper)
        return [
            remote(src, dst.at[at], w_send.at[3 * k + j], w_recv.at[3 * slot + j], w_targets[k])
            for j, (src, dst) in enumerate(w_pairs)
        ]

    for k in range(3):
        for copy in w_copies(block, k):
            copy.start()

    def to_part(src, zz):
        return remote(src, wo_v.at[2 * zz + c], part_send.at[zz], part_recv.at[zz], dev(z, 1 - c))

    def to_right(src, zz, s):
        return remote(src, wo_v.at[2 * zz + c], right_send.at[s], right_recv.at[s], dev(right, c))

    def to_left(src, zz, s):
        return remote(src, wo_v.at[2 * zz + c], left_send.at[s], left_recv.at[s], dev(left, c))

    to_right(wo_hbm, z, 0).start()
    to_left(wo_hbm, z, 0).start()
    to_part(wo_hbm, z).start()

    def from_left(s, forward):
        zz = lax.rem(z + nz - s, nz)
        mine = wo_v.at[2 * zz + c]
        to_right(mine, zz, s - 1).wait_recv()
        if forward:
            to_right(mine, zz, s).start()
        to_part(mine, zz).start()

    def from_right(s, forward):
        zz = lax.rem(z + s, nz)
        mine = wo_v.at[2 * zz + c]
        to_left(mine, zz, s - 1).wait_recv()
        if forward:
            to_left(mine, zz, s).start()
        to_part(mine, zz).start()

    def ring(first, last):
        def step(s, _):
            from_left(s, True)
            from_right(s, True)
            return 0

        lax.fori_loop(first, last + 1, step, 0)

    def wt_copy(to, slot, d):
        return remote(wt_v, wt_recv.at[slot], sendw.at[d], wt_sem.at[slot], dev(to, c))

    def wt_start(i, _):
        d = farthest_first(i, nz)
        wt_copy(lax.rem(z + d, nz), z, d).start()
        return 0

    lax.fori_loop(0, nz - 1, wt_start, 0)

    e_pairs = ((wg_hbm, wg_v), (wu_hbm, wu_v), (wd_hbm, wd_v))

    def e_copies(slot):
        return [
            remote(src.at[0], dst.at[slot], e_send.at[j], e_recv.at[j], dev(z, 1 - c))
            for j, (src, dst) in enumerate(e_pairs)
        ]

    for copy in e_copies(c):
        copy.start()

    ring(1, 3)

    for copy in local[3:6]:
        copy.wait()
    for k in range(1, 4):
        for copy in w_copies(lax.rem(block + k, 4), 0):
            copy.wait_recv()

    def p1_wait(i, _):
        d = farthest_first(i, nm)
        p1_copy(m, lax.rem(m + nm - d, nm), d).wait_recv()
        return 0

    lax.fori_loop(0, nm - 1, p1_wait, 0)

    def p1_sent(d, _):
        p1_copy(m, m, d).wait_send()
        return 0

    lax.fori_loop(1, nm, p1_sent, 0)

    x1 = p1_recv[:, 0, :].astype(BF16)
    part_q = dot(x1, wq_v[...])
    part_l = dot(x1, wl_v[...])
    part_r = dot(x1, wr_v[...])
    for i in range(nm):
        p2_send[i, :, 0:q_width] = part_q[i : i + 1, :]
        p2_send[i, :, q_width : q_width + lat] = part_l[i : i + 1, :]
        p2_send[i, :, q_width + lat : q_width + lat + ropes] = part_r[i : i + 1, :]

    def p2_copy(to, slot, d):
        return remote(p2_send.at[to], p2_recv.at[slot], send16.at[d], p2_sem.at[slot], dev(2 * to + p, c))

    def p2_start(i, _):
        d = farthest_first(i, nm)
        p2_copy(lax.rem(m + d, nm), m, d).start()
        return 0

    lax.fori_loop(0, nm - 1, p2_start, 0)

    ring(4, 8)

    def p2_wait(i, acc):
        d = nm - 1 - i
        src = lax.rem(m + nm - d, nm)
        p2_copy(m, src, d).wait_recv()
        return acc + p2_recv[src]

    summed = lax.fori_loop(0, nm - 1, p2_wait, p2_send[m])

    for copy in local[6:10]:
        copy.wait()
    query = summed[:, :q_width].astype(BF16).astype(F32)
    latent_raw = summed[:, q_width : q_width + lat].astype(BF16).astype(F32)
    rope_raw = summed[:, q_width + lat :].astype(BF16).astype(F32)
    new_latent = (
        latent_raw
        * lax.rsqrt(jnp.mean(latent_raw * latent_raw, axis=-1, keepdims=True) + EPS)
        * gain_latent_v[...]
    ).astype(BF16)
    cosine, sine = cos_v[...], sin_v[...]
    new_rope = rotate(rope_raw, cosine[:, : rope_raw.shape[1]], sine[:, : rope_raw.shape[1]]).astype(BF16)
    new_latent_ref[...] = new_latent
    new_rope_ref[...] = new_rope[:, :ropes]

    size = NOPE + ROPE
    q_nope = jnp.concatenate([query[:, h * size : h * size + NOPE] for h in range(HEADS)], axis=1)
    q_rope = jnp.concatenate([query[:, h * size + NOPE : (h + 1) * size] for h in range(HEADS)], axis=1)
    q_rope = rotate(q_rope, cosine, sine).astype(BF16).astype(F32)

    def by_head(row, width):
        shape = (HEADS, row.shape[1])
        own = lax.broadcasted_iota(jnp.int32, shape, 1) // width == lax.broadcasted_iota(jnp.int32, shape, 0)
        return jnp.where(own, jnp.broadcast_to(row, shape), 0.0)

    fold_shape = (HEADS * ROPE, ROPE)
    fold = (
        lax.rem(lax.broadcasted_iota(jnp.int32, fold_shape, 0), ROPE)
        == lax.broadcasted_iota(jnp.int32, fold_shape, 1)
    ).astype(F32).astype(BF16)
    q_pe = dot(by_head(q_rope, ROPE).astype(BF16), fold).astype(BF16)
    local[11].wait()
    q_abs = dot_nt(by_head(q_nope, NOPE).astype(BF16), wa_v[...]).astype(BF16)

    local[12].wait()
    local[13].wait()
    scale = (NOPE + ROPE) ** (-0.5)
    past = (dot_nt(q_abs, cache_v[...]) + dot(q_pe, rope_v[...])) * scale
    fresh = (
        jnp.sum(q_abs.astype(F32) * new_latent.astype(F32), axis=-1, keepdims=True)
        + jnp.sum(q_pe.astype(F32) * new_rope[:, :ropes].astype(F32), axis=-1, keepdims=True)
    ) * scale
    valid = lax.broadcasted_iota(jnp.int32, past.shape, 1) < length_ref[0]
    top = jnp.maximum(jnp.max(jnp.where(valid, past, -jnp.inf), axis=-1, keepdims=True), fresh)
    e_past = jnp.where(valid, jnp.exp(past - top), 0.0)
    e_new = jnp.exp(fresh - top)
    total = jnp.sum(e_past, axis=-1, keepdims=True) + e_new
    p_past = (e_past / total).astype(BF16)
    p_new = (e_new / total).astype(BF16).astype(F32)
    attended = (dot(p_past, cache_v[...]) + p_new * new_latent.astype(F32)).astype(BF16)
    local[14].wait()
    crossed = dot(attended, wv_v[...])
    own_head = (
        lax.broadcasted_iota(jnp.int32, crossed.shape, 1) // VDIM
        == lax.broadcasted_iota(jnp.int32, crossed.shape, 0)
    )
    values = jnp.sum(jnp.where(own_head, crossed, 0.0), axis=0, keepdims=True).astype(BF16)

    ring(9, nm - 2)
    from_left(nm - 1, True)
    from_right(nm - 1, False)
    from_left(nm, False)
    local[10].wait()

    def part_wait(zz, _):
        remote(
            wo_v.at[2 * zz + 1 - c], wo_v.at[2 * zz + 1 - c], part_send.at[zz], part_recv.at[zz], dev(z, 1 - c)
        ).wait_recv()
        return 0

    lax.fori_loop(0, nz, part_wait, 0)

    attn_out = dot(values, wo_v[...].reshape(-1, d_model))
    resid = (tokens + attn_out).astype(BF16).astype(F32)
    moe_in = resid * lax.rsqrt(jnp.mean(resid * resid, axis=-1, keepdims=True) + EPS) * gain_moe_v[...]
    moe_in = moe_in.astype(BF16).astype(F32)
    p3_send[...] = jnp.concatenate([moe_in[:, :half], moe_in[:, half:]], axis=0).astype(BF16)

    def p3_copy(to, slot, d):
        return remote(p3_send, p3_recv.at[slot], send32.at[d], p3_sem.at[slot], dev(to, c))

    def p3_start(i, _):
        d = farthest_first(i, nz)
        p3_copy(lax.rem(z + d, nz), z, d).start()
        return 0

    lax.fori_loop(0, nz - 1, p3_start, 0)
    x3[pl.ds(z, 1), :] = moe_in

    for copy in local[15:18]:
        copy.wait()
    for copy in e_copies(1 - c):
        copy.wait_recv()

    def wt_wait(i, _):
        d = i + 1
        wt_copy(z, lax.rem(z + nz - d, nz), d).wait()
        return 0

    lax.fori_loop(0, nz - 1, wt_wait, 0)

    def p3_wait(i, _):
        near = i // 2 + 1
        src = lax.rem(z + nz + near * (1 - 2 * lax.rem(i, 2)), nz)
        p3_copy(z, src, 0).wait_recv()
        row = p3_recv[src].astype(F32)
        x3[pl.ds(src, 1), 0:half] = row[0:1]
        x3[pl.ds(src, 1), half:d_model] = row[1:2]
        return 0

    lax.fori_loop(0, nz - 1, p3_wait, 0)

    def p3_sent(d, _):
        p3_copy(z, z, d).wait_send()
        return 0

    lax.fori_loop(1, nz, p3_sent, 0)

    rows3 = x3[...].astype(BF16)
    shares = wt_recv[:, 0, :]
    expert = lax.broadcasted_iota(jnp.int32, shares.shape, 1)
    outs = []
    for s in range(2):
        share = jnp.sum(jnp.where(expert == 2 * z + s, shares, 0.0), axis=1, keepdims=True)
        gate = dot(rows3, wg_v[s])
        upper = dot(rows3, wu_v[s])
        hidden = (jax.nn.silu(gate) * upper).astype(BF16)
        result = dot(hidden, wd_v[s]).astype(BF16).astype(F32)
        outs.append(share * result)
    c4[...] = outs[0] + outs[1]

    def p4_copy(to, slot, d):
        return remote(p4_send.at[to], p4_recv.at[slot], send32.at[d], p4_sem.at[slot], dev(to, c))

    def p4_start(i, _):
        d = farthest_first(i, nz)
        to = lax.rem(z + d, nz)
        row = c4[pl.ds(to, 1), :]
        p4_send[to] = jnp.concatenate([row[:, :half], row[:, half:]], axis=0).astype(BF16)
        p4_copy(to, z, d).start()
        return 0

    lax.fori_loop(0, nz - 1, p4_start, 0)
    mine = c4[pl.ds(z, 1), :]

    def p4_wait(i, acc):
        near = i // 2 + 1
        src = lax.rem(z + nz + near * (1 - 2 * lax.rem(i, 2)), nz)
        p4_copy(z, src, 0).wait_recv()
        return acc + p4_recv[src].astype(F32)

    acc = lax.fori_loop(
        0, nz - 1, p4_wait, jnp.concatenate([mine[:, :half], mine[:, half:]], axis=0)
    )
    mixed_ref[:, :half] = (resid[:, :half] + acc[0:1]).astype(BF16)
    mixed_ref[:, half:] = (resid[:, half:] + acc[1:2]).astype(BF16)

    def p4_sent(d, _):
        p4_copy(z, z, d).wait_send()
        return 0

    lax.fori_loop(1, nz, p4_sent, 0)

    def p2_sent(d, _):
        p2_copy(m, m, d).wait_send()
        return 0

    lax.fori_loop(1, nm, p2_sent, 0)
    for k in range(3):
        for copy in w_copies(block, k):
            copy.wait_send()
    for copy in e_copies(c):
        copy.wait_send()

    def ring_sent(s, _):
        to_right(wo_v.at[e], z, s).wait_send()
        return 0

    lax.fori_loop(0, nm, ring_sent, 0)

    def ring_sent_left(s, _):
        to_left(wo_v.at[e], z, s).wait_send()
        return 0

    lax.fori_loop(0, nm - 1, ring_sent_left, 0)

    def part_sent(zz, _):
        to_part(wo_v.at[e], zz).wait_send()
        return 0

    lax.fori_loop(0, nz, part_sent, 0)


def solution(mesh):
    n = mesh.shape["ep"]
    nz = n // 2
    nm = nz // 2

    def body(
        tokens,
        cache_latent,
        cache_rope,
        lengths,
        w_query,
        w_latent,
        w_rope,
        w_absorb,
        w_value,
        w_output,
        gain_attn,
        gain_latent,
        gain_moe,
        routes,
        route_scores,
        w_gate,
        w_up,
        w_down,
    ):
        d = tokens.shape[1]
        cosine, sine = rope_tables(lengths, ROPE)
        cosine = jnp.tile(cosine, (1, 2 * HEADS))
        sine = jnp.tile(sine, (1, 2 * HEADS))
        route_weight = route_scores / jnp.sum(route_scores, axis=-1, keepdims=True)
        lanes = max(128, n)
        hits = routes[:, :, None] == jnp.arange(lanes)[None, None, :]
        table = jnp.sum(hits.astype(F32) * route_weight[:, :, None], axis=1)

        fper = w_query.shape[0]
        feats = 4 * fper
        width = w_query.shape[1] + w_latent.shape[1]
        wide = width + 128
        ff = w_gate.shape[2]
        inputs = (
            lengths,
            tokens,
            cache_latent,
            cache_rope,
            w_query,
            w_latent,
            w_rope,
            w_absorb,
            w_value,
            w_output,
            gain_attn[None, :],
            gain_latent[None, :],
            gain_moe[None, :],
            cosine,
            sine,
            table,
            w_gate,
            w_up,
            w_down,
        )
        dma = pltpu.SemaphoreType.DMA
        return pl.pallas_call(
            functools.partial(kernel, nz),
            out_shape=(
                jax.ShapeDtypeStruct((1, d), BF16),
                jax.ShapeDtypeStruct((1, LATENT), BF16),
                jax.ShapeDtypeStruct((1, ROPE), BF16),
            ),
            in_specs=[pl.BlockSpec(memory_space=pltpu.SMEM)]
            + [pl.BlockSpec(memory_space=pl.ANY)] * (len(inputs) - 1),
            out_specs=(pl.BlockSpec(memory_space=pltpu.VMEM),) * 3,
            scratch_shapes=[
                pltpu.VMEM((1, d), BF16),
                pltpu.VMEM((1, d), F32),
                pltpu.VMEM((1, LATENT), F32),
                pltpu.VMEM((1, d), F32),
                pltpu.VMEM(cosine.shape, F32),
                pltpu.VMEM(sine.shape, F32),
                pltpu.VMEM((1, lanes), F32),
                pltpu.VMEM(cache_latent.shape[1:], BF16),
                pltpu.VMEM(cache_rope.shape[1:], BF16),
                pltpu.VMEM(w_absorb.shape, BF16),
                pltpu.VMEM(w_value.shape, BF16),
                pltpu.VMEM((feats, w_query.shape[1]), BF16),
                pltpu.VMEM((feats, w_latent.shape[1]), BF16),
                pltpu.VMEM((feats, w_rope.shape[1]), BF16),
                pltpu.VMEM((n,) + w_output.shape, BF16),
                pltpu.VMEM((2, d, ff), BF16),
                pltpu.VMEM((2, d, ff), BF16),
                pltpu.VMEM((2, ff, d), BF16),
                pltpu.VMEM((nm, 1, feats), F32),
                pltpu.VMEM((nm, 1, feats), F32),
                pltpu.VMEM((nz, 1, lanes), F32),
                pltpu.VMEM((nm, 1, wide), F32),
                pltpu.VMEM((nm, 1, wide), F32),
                pltpu.VMEM((2, d // 2), BF16),
                pltpu.VMEM((nz, 2, d // 2), BF16),
                pltpu.VMEM((nz, d), F32),
                pltpu.VMEM((nz, d), F32),
                pltpu.VMEM((nz, 2, d // 2), BF16),
                pltpu.VMEM((nz, 2, d // 2), BF16),
                dma((18,)),
                dma((nm,)),
                dma((nz,)),
                dma((nz,)),
                dma((nm,)),
                dma((nz,)),
                dma((nm,)),
                dma((nz,)),
                dma((nz,)),
                dma((9,)),
                dma((12,)),
                dma((3,)),
                dma((3,)),
                dma((nm,)),
                dma((nm,)),
                dma((nm,)),
                dma((nm,)),
                dma((nz,)),
                dma((nz,)),
            ],
            compiler_params=pltpu.CompilerParams(
                collective_id=0, has_side_effects=True, vmem_limit_bytes=60 * 1024 * 1024
            ),
        )(*inputs)

    rows = P(("grp", "ep"), None)
    cached = P(("grp", "ep"), None, None)
    held = P("ep", None)
    experts = P("ep", None, None)
    return jax.shard_map(
        body,
        mesh=mesh,
        in_specs=(
            rows,
            cached,
            cached,
            P(("grp", "ep")),
            held,
            held,
            held,
            P(),
            P(),
            held,
            P(),
            P(),
            P(),
            rows,
            rows,
            experts,
            experts,
            experts,
        ),
        out_specs=(rows, rows, rows),
        check_vma=False,
    )
```

time: 369 us -> 156 us (0.42)
  waiting for transfers between devices: 196 us -> 0 us
  Pallas kernels: 0 us -> 145 us
  blocking collectives: 83.7 us -> 0 us
  starting transfers between devices: 37.1 us -> 0 us
  matrix products: 13.9 us -> 0 us
  other arithmetic: 17.7 us -> 3.87 us
  local copies, waits for them, and re-layouts: 15.3 us -> 5.02 us
    all_to_all x5 -> x0, waiting for transfers between devices: 196 us -> none  [the longest x1 61.8 us: summed_on_arrival(): lax.all_to_all(tiles, axis, split_axis=0, concat_axis=0, tiled=True)]
    pallas_call x0 -> x1, Pallas kernels: none -> 145 us  [body(): pl.pallas_call(functools.partial(kernel, nz), out_shape=(jax.ShapeDtypeSt...]
    all_to_all x2 -> x0, blocking collectives: 83.7 us -> none  [the longest x1 56 us: body(): lax.all_to_all(normed, 'ep', split_axis=1, concat_axis=0, tiled=True)]
    all_to_all x5 -> x0, starting transfers between devices: 37.1 us -> none  [the longest x1 10.3 us: body(): lax.all_to_all(outgoing, 'ep', split_axis=0, concat_axis=0, tiled=True)]
    dot_general x14 -> x0, matrix products: 13.9 us -> none  [the longest x1 2.98 us: body(): jnp.dot(hidden, w_down[0], preferred_element_type=jnp.float32)]
    unnamed x28 -> x3, local copies, waits for them, and re-layouts: 12.2 us -> 3.69 us
    reduce_sum x7 -> x1, other arithmetic: 5.95 us -> 1.25 us  [body(): table = jnp.sum(hits.astype(F32) * route_weight[:, :, None], axis=1)]
    select_n x2 -> x0, other arithmetic: 4.36 us -> none  [body(): jnp.where(chosen.T[:, :, None], moe_in[None, :, :], jnp.zeros((), jnp.bfl...]
  transfers between devices with their start and end apart: 5 -> 0, of which waited for: 5 -> 0; matrix products, arithmetic and copies ran while one was open for 5% -> 0% of each run, Pallas kernels for 0% -> 0%
where the time goes in v1:
time: 156 us; the launch traced here: 155 us
  Pallas kernels  145 us (93%)
  local copies, waits for them, and re-layouts  5.02 us (3%)
  other arithmetic  3.87 us (2%)
    pallas_call x1, Pallas kernels, body(): pl.pallas_call(functools.partial(kernel, nz), out_shape=(jax.ShapeDtypeSt...  145 us
    unnamed x3, local copies, waits for them, and re-layouts  3.69 us

profile of v1, /device:TPU:46, one launch (start us, length us, event | category | flops | bytes accessed | tf_op | source)
XLA Modules:
  0.0 154.7 jit_solution(17526261684598557412)
XLA Ops:
  1.3 0.7 tile.21.sin_hbm
  2.0 0.7 tile.9.cos_hbm
  2.7 1.3 reduce_sum.20
  3.9 1.3 divide_bitcast_fusion
  5.2 1.3 fusion
  6.5 144.5 %shard_map.196 = (bf16[1,2048]{1,0:T(2,128)(2,1)}, bf16[1,512]{1,0:T(2,128)(2,1)}, bf16[1,32]{1,0:T(2,128)(2,1)}) custom-call(s32[1]{0:T(128)S(6)} %copy.24.length_ref, bf16[1,2048]{1,0:T(2,128)(2,1)} %tokens_hbm.1, bf16[1,3072,512]{2,1,0:T(8,128)(2,1)} %cache_hbm.1, bf16[1,32,3072]{2,1,0:T(8,128)(2,1)} %rope_hbm.1, bf16[32,1536]{1,0:T(8,128)(2,1)} %wq_hbm.1, ...), custom_call_target="tpu_custom_call" | custom-call | tf_op jit(solution)/shard_map/pallas_call | solution.py:586
  151.0 1.3 copy.25
  152.3 1.3 copy.26
  153.6 1.1 copy.27
  (3 shorter events, 0.1 us)
